TPU v7x, 32 devices: a whole 2x2x4 slice. The times are simulated.
32 devices in a mesh: ep: 4 (over y, x), tp: 8 (over z, core).
Axes of the slice: x: 2, y: 2, z: 4, core: 2. Of those that a mesh axis runs over, the one named last changes fastest.
Arguments:
- tokens: bfloat16 [256, 4096], P(('ep', 'tp')), may hold values from -6 to 6
- rec_state: float32 [256, 2048], P('ep', 'tp'), may hold values from -40 to 40
- conv_state: bfloat16 [256, 3, 2048], P('ep', None, 'tp'), may hold values from -6 to 6
- route_ids: int32 [256, 4], P('ep'), may hold values from 0 to 15, all different within a row; in each aligned block of 8 rows (0 to 7, 8 to 15, ...) at most 2 rows name the same one
- route_weights: float32 [256, 4], P(('ep', 'tp')), may hold values from 0.1 to 1
- first_gain: bfloat16 [4096], replicated, may hold values from 0.099609375 to 1.8984375
- proj_input: bfloat16 [4096, 2048], P(None, 'tp'), may hold values from -0.09375 to 0.09375
- proj_gate: bfloat16 [4096, 2048], P(None, 'tp'), may hold values from -0.09375 to 0.09375
- conv_taps: bfloat16 [4, 2048], replicated, may hold values from -1.5 to 1.5
- decay_logit: float32 [2048], replicated, may hold values from 1 to 6
- block_decay: bfloat16 [16, 128, 128], replicated, may hold values from -0.5 to 0.5
- block_input: bfloat16 [16, 128, 128], replicated, may hold values from -0.5 to 0.5
- rec_gain: bfloat16 [2048], replicated, may hold values from 0.099609375 to 1.8984375
- proj_out: bfloat16 [2048, 4096], P('tp'), may hold values from -0.125 to 0.125
- second_gain: bfloat16 [4096], replicated, may hold values from 0.099609375 to 1.8984375
- expert_gate: bfloat16 [16, 4096, 4096], P('ep', None, 'tp'), may hold values from -0.21875 to 0.21875
- expert_up: bfloat16 [16, 4096, 4096], P('ep', None, 'tp'), may hold values from -0.21875 to 0.21875
- expert_down: bfloat16 [16, 4096, 4096], P('ep', 'tp'), may hold values from -0.0234375 to 0.0234375
Outputs:
- result: bfloat16 [256, 4096], P(('ep', 'tp'))
- new_state: float32 [256, 2048], P('ep', 'tp')
- new_conv: bfloat16 [256, 3, 2048], P('ep', None, 'tp')
Inputs may be any that keep to these rules, and one draw needn't show every extreme that they name: `route_ids`: each row names 4 different experts; in the rows of one device (aligned blocks of 8 rows) no expert is named by more than 2 rows, and one is named by exactly 2.
All inputs are finite; a program needn't handle non-finite values.
Results may differ from a plain program's by a relative error of at most 0.025.
Values may be sent and summed in bfloat16 or wider, within the bound.
A program may use at most 128 MiB of HBM per device.

v0:
```python
import jax
import jax.numpy as jnp
from jax import lax
from jax.sharding import PartitionSpec as P

EXPERTS = 16


EPS = 1e-06
CLAMP = 7.0
ALPHA = 1.702
RATE = 8.0


def norm_rows(values, gain):
    scale = lax.rsqrt(jnp.mean(values * values, axis=-1, keepdims=True) + EPS)
    return values * scale * gain.astype(jnp.float32)


def slot_positions(ids, blocks):
    rows, picks = ids.shape
    onehot = (ids[:, :, None] == jnp.arange(EXPERTS, dtype=jnp.int32)).astype(jnp.int32)
    onehot = onehot.reshape(blocks, rows // blocks * picks, EXPERTS)
    before = jnp.cumsum(onehot, axis=1) - onehot
    return jnp.sum(before * onehot, axis=-1).reshape(rows, picks)


def dispatch_rows(slots, rows_in, total):
    hits = (slots[:, :, None] == jnp.arange(total, dtype=jnp.int32)).astype(jnp.bfloat16)
    chooser = jnp.sum(hits, axis=1)
    return jnp.einsum("ns,nd->sd", chooser, rows_in, preferred_element_type=jnp.float32).astype(
        jnp.bfloat16
    )


def run_experts(piece, expert_gate, expert_up, expert_down):
    gate = jnp.einsum("erd,edf->erf", piece, expert_gate, preferred_element_type=jnp.float32)
    upper = jnp.einsum("erd,edf->erf", piece, expert_up, preferred_element_type=jnp.float32)
    clipped = jnp.minimum(gate, CLAMP)
    act = (
        (jnp.clip(upper, -CLAMP, CLAMP) + 1.0) * (clipped * jax.nn.sigmoid(ALPHA * clipped))
    ).astype(jnp.bfloat16)
    return jnp.einsum("erf,efd->erd", act, expert_down, preferred_element_type=jnp.float32)


def per_device(
    tokens,
    rec_state,
    conv_state,
    route_ids,
    route_weights,
    first_gain,
    proj_input,
    proj_gate,
    conv_taps,
    decay_logit,
    block_decay,
    block_input,
    rec_gain,
    proj_out,
    second_gain,
    expert_gate,
    expert_up,
    expert_down,
):
    tp_count = lax.axis_size("tp")
    tp_place = lax.axis_index("tp")
    local_width = proj_input.shape[1]
    seq_count = rec_state.shape[0]
    own_count = tokens.shape[0]
    top_count = route_ids.shape[1]
    capacity = max(2, own_count * top_count // EXPERTS)
    first_channel = tp_place * local_width
    own_values = tokens.astype(jnp.float32)
    normed = norm_rows(own_values, first_gain).astype(jnp.bfloat16)
    piece = lax.all_gather(normed, "tp", axis=0, tiled=True)
    both = jnp.concatenate(
        [
            jnp.dot(piece, proj_input, preferred_element_type=jnp.float32),
            jnp.dot(piece, proj_gate, preferred_element_type=jnp.float32),
        ],
        axis=1,
    )
    joined = both.astype(jnp.bfloat16)
    branch_in = joined[:, :local_width]
    branch_gate = joined[:, local_width:]
    tap_weights = lax.dynamic_slice_in_dim(conv_taps, first_channel, local_width, 1).astype(
        jnp.float32
    )
    conv_values = conv_state.astype(jnp.float32)
    conv_output = tap_weights[-1] * branch_in.astype(jnp.float32)
    for tap in range(conv_state.shape[1]):
        conv_output = conv_output + tap_weights[tap] * conv_values[:, tap]
    new_conv = jnp.concatenate([conv_state[:, 1:], branch_in[:, None, :]], axis=1)
    block_width = block_decay.shape[1]
    local_blocks = local_width // block_width
    decay_mats = lax.dynamic_slice_in_dim(block_decay, tp_place * local_blocks, local_blocks, 0)
    input_mats = lax.dynamic_slice_in_dim(block_input, tp_place * local_blocks, local_blocks, 0)
    blocked = conv_output.astype(jnp.bfloat16).reshape(seq_count, local_blocks, block_width)
    decay_gate = jax.nn.sigmoid(
        jnp.einsum("rnk,nkj->rnj", blocked, decay_mats, preferred_element_type=jnp.float32).reshape(
            seq_count, local_width
        )
    )
    input_gate = jax.nn.sigmoid(
        jnp.einsum("rnk,nkj->rnj", blocked, input_mats, preferred_element_type=jnp.float32).reshape(
            seq_count, local_width
        )
    )
    decay_logits = lax.dynamic_slice_in_dim(decay_logit, first_channel, local_width, 0)
    log_keep = -RATE * decay_gate * jax.nn.softplus(-decay_logits)
    keep_factor = jnp.exp(log_keep)
    fresh_input = jnp.sqrt(-jnp.expm1(2.0 * log_keep)) * input_gate * conv_output
    new_state = keep_factor * rec_state + fresh_input
    hidden = new_state * jax.nn.gelu(branch_gate.astype(jnp.float32))
    squares = jnp.sum(hidden * hidden, axis=1, keepdims=True)
    gain_part = lax.dynamic_slice_in_dim(rec_gain, first_channel, local_width, 0).astype(
        jnp.float32
    )
    partial_value = jnp.dot(
        (hidden * gain_part).astype(jnp.bfloat16), proj_out, preferred_element_type=jnp.float32
    )
    channels = local_width * tp_count
    width_out = proj_out.shape[1]
    own_ids = lax.dynamic_slice_in_dim(route_ids, tp_place * own_count, own_count, 0)
    own_slots = own_ids * capacity + slot_positions(own_ids, 1)
    mix_part, own_squares = (
        lax.psum_scatter(
            partial_value.astype(jnp.bfloat16), "tp", scatter_dimension=0, tiled=True
        ).astype(jnp.float32),
        lax.psum_scatter(
            squares.astype(jnp.bfloat16), "tp", scatter_dimension=0, tiled=True
        ).astype(jnp.float32),
    )
    residual = own_values + mix_part * lax.rsqrt(own_squares / channels + EPS)
    second_normed = norm_rows(residual, second_gain).astype(jnp.bfloat16)
    outgoing = dispatch_rows(own_slots, second_normed, EXPERTS * capacity).reshape(
        EXPERTS, capacity, width_out
    )
    arrived = lax.all_to_all(outgoing, "ep", split_axis=0, concat_axis=1, tiled=True)
    partials = run_experts(
        lax.all_gather(arrived, "tp", axis=1, tiled=True), expert_gate, expert_up, expert_down
    )
    summed_rows = lax.psum_scatter(
        partials.astype(jnp.bfloat16), "tp", scatter_dimension=1, tiled=True
    )
    returned = lax.all_to_all(summed_rows, "ep", split_axis=1, concat_axis=0, tiled=True)
    returned_rows = returned.reshape(EXPERTS * capacity, width_out).astype(jnp.float32)
    slot_hits = (own_slots[:, :, None] == jnp.arange(EXPERTS * capacity, dtype=jnp.int32)).astype(
        jnp.float32
    )
    combine_weights = jnp.sum(slot_hits * route_weights[:, :, None], axis=1)
    expert_mix = jnp.dot(combine_weights, returned_rows, precision=lax.Precision.HIGHEST)
    result = (residual + expert_mix).astype(jnp.bfloat16)
    return (result, new_state, new_conv)


def solution(mesh):
    in_specs = (
        P(("ep", "tp"), None),
        P("ep", "tp"),
        P("ep", None, "tp"),
        P("ep", None),
        P(("ep", "tp"), None),
        P(),
        P(None, "tp"),
        P(None, "tp"),
        P(),
        P(),
        P(),
        P(),
        P(),
        P("tp", None),
        P(),
        P("ep", None, "tp"),
        P("ep", None, "tp"),
        P("ep", "tp", None),
    )
    out_specs = (P(("ep", "tp"), None), P("ep", "tp"), P("ep", None, "tp"))
    return jax.shard_map(
        per_device, mesh=mesh, in_specs=in_specs, out_specs=out_specs, check_vma=False
    )
```

profile of v0, /device:TPU:0, one launch (start us, length us, event | category | flops | bytes accessed | tf_op | source)
XLA Modules:
  0.0 196.3 jit_solution(4809331061785495694)
XLA Ops:
  7.2 0.0 copy-start
  7.2 0.0 reduce-scatter.6.cloned.1.call-start
  7.2 0.8 dynamic-slice_convert_fusion
  8.1 0.7 convert_element_type.98
  8.8 1.0 fusion.17
  9.8 0.9 fusion.19
  10.7 16.5 %all_gather.6 = bf16[64,4096]{1,0:T(8,128)(2,1)S(1)} all-gather(bf16[8,4096]{1,0:T(8,128)(2,1)S(1)} %fusion.19), channel_id=1, replica_groups=mesh['ep'=4,'tp'=8] {'tp'}, dimensions={0}, use_global_device_ids=true | all-gather | bytes 589824 | tf_op jit(solution)/shard_map/all_gather | solution.py:76
  27.2 0.9 convert_element_type.101
  28.1 2.1 %convolution_convert_fusion.4 = bf16[64,256]{1,0:T(8,128)(2,1)S(1)} fusion(bf16[64,4096]{1,0:T(8,128)(2,1)S(1)} %all_gather.6, bf16[4096,256]{1,0:T(8,128)(2,1)} %param.24), kind=kOutput, calls=%fused_computation.22 | convolution fusion | flops 134234112 | bytes 2654208 | tf_op jit(solution)/shard_map/dot_general | solution.py:79
  30.2 1.0 fusion.11
  31.2 1.0 fusion.7
  32.2 0.8 fusion.49
  33.0 0.8 dynamic-slice_convert_fusion.2
  33.8 0.1 fusion.29
  33.9 0.0 copy-start.5
  33.9 2.2 %multiply_reduce_fusion.1 = (bf16[64]{0:T(256)(128)(2,1)S(1)}, f32[64,256]{1,0:T(8,128)S(1)}) fusion(f32[64,256]{1,0:T(8,128)S(1)} %fusion.29, bf16[64,4096]{1,0:T(8,128)(2,1)S(1)} %all_gather.6, bf16[4096,256]{1,0:T(8,128)(2,1)} %param.25), kind=kOutput, calls=%fused_computation.63 | convolution fusion | flops 134430656 | bytes 2752640 | tf_op jit(solution)/shard_map/dot_general | solution.py:80
  36.1 0.0 copy-start.8
  36.1 0.0 copy-start.7
  36.1 0.0 copy-start.10
  36.1 0.0 copy-start.3
  36.1 0.0 copy-done
  36.1 1.3 convolution_convert_fusion.1
  37.4 0.0 copy-done.5
  37.4 0.0 reduce-scatter.6.cloned.1.call-update
  37.4 0.0 all-gather.2.cloned.1.call-start
  37.5 0.1 constant_dynamic-slice_fusion
  37.6 0.1 copy.58
  37.7 0.1 eq.49
  37.7 0.1 fusion.47
  37.8 0.1 reduce_window_sum.11
  37.9 0.2 select_reduce_fusion.1
  38.1 0.1 reshape.160
  38.1 0.1 copy.50
  38.2 0.0 copy-done.7
  38.2 0.0 copy-done.10
  38.3 0.6 dynamic-slice
  39.5 17.0 %all-reduce = bf16[64,1]{0,1:T(2,128)(2,1)S(1)} all-reduce(bf16[64,1]{0,1:T(2,128)(2,1)S(1)} %bitcast.97), channel_id=3, replica_groups=mesh['ep'=4,'tp'=8] {'tp'}, use_global_device_ids=true, to_apply=%region_3.4.clone | all-reduce | flops 64 | bytes 256
  56.5 0.1 rsqrt_bitcast_fusion
  56.6 0.1 fusion.48
  56.6 13.2 %reduce-scatter.6.cloned.1.call-done = bf16[8,4096]{1,0:T(8,128)(2,1)} async-done(((bf16[64,4096]{1,0:T(8,128)(2,1)}), bf16[8,4096]{1,0:T(8,128)(2,1)}) %reduce-scatter.6.cloned.1.call-update) | async-done | bytes 65552 | tf_op jit(solution)/shard_map/reduce_scatter | solution.py:128
  69.9 1.1 multiply_reduce_fusion
  71.0 1.1 convolution_convert_fusion.2
  72.1 0.2 reshape.161
  72.3 9.2 %all_to_all.33 = bf16[16,2,4096]{2,1,0:T(2,128)(2,1)S(1)} all-to-all(bf16[16,2,4096]{2,1,0:T(2,128)(2,1)S(1)} %reshape.161), channel_id=1, replica_groups=mesh['ep'=4,'tp'=8] {'ep'}, dimensions={0} | all-to-all | bytes 524288 | tf_op jit(solution)/shard_map/all_to_all | solution.py:140
  81.5 0.2 copy.78
  81.7 0.8 all_to_all.27
  82.5 0.0 all-gather.2.cloned.1.call-update
  82.5 0.2 reduce-scatter.8.cloned.1.call-start
  82.7 26.3 %all-gather.2.cloned.1.call-done = bf16[4,64,4096]{2,1,0:T(8,128)(2,1)} async-done(((bf16[4,8,4096]{2,1,0:T(8,128)(2,1)}), bf16[4,64,4096]{2,1,0:T(8,128)(2,1)}) %all-gather.2.cloned.1.call-update) | async-done | bytes 2097168 | tf_op jit(solution)/shard_map/all_gather | solution.py:142
  109.0 9.5 %convolution_minimum_fusion = f32[4,64,512]{2,1,0:T(8,128)S(1)} fusion(bf16[4,64,4096]{2,1,0:T(8,128)(2,1)} %all-gather.2.cloned.1.call-done, bf16[4,4096,512]{2,1,0:T(8,128)(2,1)} %param.33), kind=kOutput, calls=%fused_computation.5 | convolution fusion | flops 1073872896 | bytes 19398656 | tf_op jit(solution)/shard_map/erd,edf->erf/dot_general | solution.py:37
  118.6 17.8 %convolution_convert_fusion = bf16[4,64,4096]{2,1,0:T(8,128)(2,1)} fusion(bf16[4,512,4096]{2,1,0:T(8,128)(2,1)} %param.35, bf16[4,64,4096]{2,1,0:T(8,128)(2,1)S(1)} %copy-done.2, bf16[4,4096,512]{2,1,0:T(8,128)(2,1)} %param.34, f32[4,64,512]{2,1,0:T(8,128)S(1)} %convolution_minimum_fusion), kind=kOutput, calls=%fused_computation | convolution fusion | flops 2149711872 | bytes 38273024 | tf_op jit(solution)/shard_map/erf,efd->erd/dot_general | solution.py:43
  136.4 3.2 %copy.56 = bf16[4,64,4096]{2,0,1:T(4,128)(2,1)S(1)} copy(bf16[4,64,4096]{2,1,0:T(8,128)(2,1)} %convolution_convert_fusion) | data formatting | bytes 4194304
  139.6 2.6 %copy.62 = bf16[8,8,4,4096]{3,1,2,0:T(8,128)(2,1)} copy(bf16[8,8,4,4096]{3,2,1,0:T(4,128)(2,1)S(1)} %bitcast.87) | data formatting | bytes 4194304
  142.2 0.0 reduce-scatter.8.cloned.1.call-update
  142.2 35.6 %reduce-scatter.8.cloned.1.call-done = bf16[8,16384]{1,0:T(8,128)(2,1)} async-done(((bf16[64,16384]{1,0:T(8,128)(2,1)}), bf16[8,16384]{1,0:T(8,128)(2,1)}) %reduce-scatter.8.cloned.1.call-update) | async-done | bytes 262160
  177.8 1.8 reshape.166
  179.6 3.5 %all-to-all-start.1 = ((bf16[4,8,4096]{2,0,1:T(4,128)(2,1)}), bf16[4,8,4096]{2,0,1:T(4,128)(2,1)S(1)}, u32[]{:S(2)}, u32[]{:S(2)}) async-start(bf16[4,8,4096]{2,0,1:T(4,128)(2,1)} %bitcast.19), calls=%async_computation.2 | async-start | bytes 524288 | tf_op jit(solution)/shard_map/all_to_all | solution.py:147
  183.1 0.7 pad_maximum_fusion
  183.8 0.1 select_reduce_fusion
  183.9 4.6 %all-to-all-done.1 = bf16[4,8,4096]{2,0,1:T(4,128)(2,1)S(1)} async-done(((bf16[4,8,4096]{2,0,1:T(4,128)(2,1)}), bf16[4,8,4096]{2,0,1:T(4,128)(2,1)S(1)}, u32[]{:S(2)}, u32[]{:S(2)}) %all-to-all-start.1) | async-done | bytes 262176 | tf_op jit(solution)/shard_map/all_to_all | solution.py:147
  188.5 0.3 copy.77
  188.8 0.1 reshape.162
  188.9 0.0 copy-done.4
  188.9 0.9 fusion
  (19 shorter events, 0.1 us)
Async XLA Ops:
  7.2 29.0 %copy-start = (bf16[256,4096]{1,0:T(8,128)(2,1)S(1)}, bf16[256,4096]{1,0:T(8,128)(2,1)}, u32[]{:S(2)}) copy-start(bf16[256,4096]{1,0:T(8,128)(2,1)} %param.31) | copy-start | bytes 6291460
  7.2 62.7 %reduce-scatter.6.cloned.1.call-start = ((), (), s32[]{:S(2)}) async-start(), calls=%async_computation.4 | async-start | bytes 589824 | tf_op jit(solution)/shard_map/reduce_scatter | solution.py:128
  27.2 6.6 %copy-start.6 = (f32[64,256]{1,0:T(8,128)S(1)}, f32[64,256]{1,0:T(8,128)}, u32[]{:S(2)}) copy-start(f32[64,256]{1,0:T(8,128)} %param.19) | copy-start | bytes 196612
  33.9 3.6 %copy-start.5 = (f32[64,256]{1,0:T(8,128)}, f32[64,256]{1,0:T(8,128)S(1)}, u32[]{:S(2)}) copy-start(f32[64,256]{1,0:T(8,128)S(1)} %fusion.29) | copy-start | bytes 196612
  36.1 1.4 copy-start.8
  36.1 2.1 %copy-start.7 = (bf16[4096]{0:T(1024)(128)(2,1)S(1)}, bf16[4096]{0:T(1024)(128)(2,1)}, u32[]{:S(2)}) copy-start(bf16[4096]{0:T(1024)(128)(2,1)} %param.32) | copy-start | bytes 24580
  36.1 2.1 %copy-start.10 = (u32[32]{0:T(128)S(1)}, u32[32]{0:T(128)}, u32[]{:S(2)}) copy-start(u32[32]{0:T(128)} %constant.63) | copy-start | bytes 388
  36.1 33.8 %copy-start.3 = (bf16[8,4096]{1,0:T(8,128)(2,1)S(1)}, bf16[8,4096]{1,0:T(8,128)(2,1)}, u32[]{:S(2)}) copy-start(bf16[8,4096]{1,0:T(8,128)(2,1)} %param.18) | copy-start | bytes 196612
  37.4 71.6 %all-gather.2.cloned.1.call-start = ((), (), s32[]{:S(2)}) async-start(), calls=%async_computation.5 | async-start | bytes 2359296 | tf_op jit(solution)/shard_map/all_gather | solution.py:142
  82.5 95.3 %reduce-scatter.8.cloned.1.call-start = ((), (), s32[]{:S(2)}) async-start(), calls=%async_computation.6 | async-start | bytes 2359296
  109.0 9.5 %copy-start.2 = (bf16[4,64,4096]{2,1,0:T(8,128)(2,1)S(1)}, bf16[4,64,4096]{2,1,0:T(8,128)(2,1)}, u32[]{:S(2)}) copy-start(bf16[4,64,4096]{2,1,0:T(8,128)(2,1)} %all-gather.2.cloned.1.call-done) | copy-start | bytes 6291460
  142.1 41.0 %slice-start = ((bf16[64,3,256]{2,0,1:T(8,128)(2,1)}), bf16[64,2,256]{2,0,1:T(8,128)(2,1)S(1)}, s32[]{:S(2)}) async-start(bf16[64,3,256]{2,0,1:T(8,128)(2,1)} %param.20), calls=%async_computation.7 | async-start | bytes 131072 | tf_op jit(solution)/shard_map/slice | solution.py:94
  142.1 41.6 %copy-start.9 = (f32[8,4]{0,1:T(4,128)S(1)}, f32[8,4]{0,1:T(4,128)}, u32[]{:S(2)}) copy-start(f32[8,4]{0,1:T(4,128)} %param.22) | copy-start | bytes 388
  142.1 47.6 %copy-start.1 = (bf16[256,4096]{1,0:T(8,128)(2,1)S(1)}, bf16[256,4096]{1,0:T(8,128)(2,1)}, u32[]{:S(2)}) copy-start(bf16[256,4096]{1,0:T(8,128)(2,1)} %param.31) | copy-start | bytes 6291460
  142.1 46.7 %copy-start.4 = (bf16[8,4096]{1,0:T(8,128)(2,1)S(1)}, bf16[8,4096]{1,0:T(8,128)(2,1)}, u32[]{:S(2)}) copy-start(bf16[8,4096]{1,0:T(8,128)(2,1)} %reduce-scatter.6.cloned.1.call-done) | copy-start | bytes 196612
  179.6 8.9 %all-to-all-start.1 = ((bf16[4,8,4096]{2,0,1:T(4,128)(2,1)}), bf16[4,8,4096]{2,0,1:T(4,128)(2,1)S(1)}, u32[]{:S(2)}, u32[]{:S(2)}) async-start(bf16[4,8,4096]{2,0,1:T(4,128)(2,1)} %bitcast.19), calls=%async_computation.2 | async-start | bytes 524288 | tf_op jit(solution)/shard_map/all_to_all | solution.py:147
Sparse Core Ops, SparseCore 0:
  37.6 32.2 reduce-scatter.5
  82.6 26.3 all-gather.1
  142.3 35.4 reduce-scatter.7
where the time goes:
time: 197 us; the launch traced here: 196 us
  waiting for transfers between devices  79.8 us (41%)
  blocking collectives  42.7 us (22%)
  matrix products  36.8 us (19%)
  between operations  14.6 us (7%)
  local copies, waits for them, and re-layouts  10.3 us (5%)
  other arithmetic  8.29 us (4%)
  starting transfers between devices  3.84 us (2%)
    unnamed x4, waiting for transfers between devices  35.6 us
    all_gather x1, waiting for transfers between devices, per_device(): lax.all_gather(arrived, 'tp', axis=1, tiled=True)  26.3 us
    dot_general x1, matrix products, run_experts(): jnp.einsum('erf,efd->erd', act, expert_down, preferred_element_type=jnp.f...  17.8 us
    unnamed x1, blocking collectives  17 us
    all_gather x1, blocking collectives, per_device(): piece = lax.all_gather(normed, 'tp', axis=0, tiled=True)  16.5 us
    reduce_scatter x1, waiting for transfers between devices, per_device(): lax.psum_scatter(partial_value.astype(jnp.bfloat16), 'tp', scatter_dimens...  13.2 us
    dot_general x1, matrix products, run_experts(): jnp.einsum('erd,edf->erf', piece, expert_gate, preferred_element_type=jnp...  9.51 us
    all_to_all x1, blocking collectives, per_device(): lax.all_to_all(outgoing, 'ep', split_axis=0, concat_axis=1, tiled=True)  9.19 us
  transfers between devices with their start and end apart: 4, of which 4 were waited for; matrix products, arithmetic and copies ran while one was open for 1% of the time, Pallas kernels for 0%

commit v1 on v0

--- a/solution.py
+++ b/solution.py
@@ -1,6 +1,10 @@
+import functools
+
 import jax
 import jax.numpy as jnp
 from jax import lax
+from jax.experimental import pallas as pl
+from jax.experimental.pallas import tpu as pltpu
 from jax.sharding import PartitionSpec as P
 
 EXPERTS = 16
@@ -43,7 +47,7 @@
     return jnp.einsum("erf,efd->erd", act, expert_down, preferred_element_type=jnp.float32)
 
 
-def per_device(
+def collective_plan(
     tokens,
     rec_state,
     conv_state,
@@ -155,6 +159,557 @@
     return (result, new_state, new_conv)
 
 
+MESH = pl.DeviceIdType.MESH
+LANES = 128
+VMEM_LIMIT = 66_900_000
+CHUNKS = 4
+
+
+def places(z_count):
+    ep, tp = lax.axis_index("ep"), lax.axis_index("tp")
+    return ep, tp // 2, tp % 2
+
+
+def remote(src, dst, send_sem, recv_sem, ep, z, core):
+    return pltpu.make_async_remote_copy(
+        src_ref=src, dst_ref=dst, send_sem=send_sem, recv_sem=recv_sem,
+        device_id=(ep, z * 2 + core), device_id_type=MESH,
+    )
+
+
+def rows16(index, count=1):
+    return pl.ds(pl.multiple_of(index * 16, 16), 16 * count)
+
+
+def fold(values):
+    half = values.shape[1] // 2
+    return jnp.concatenate([values[:, :half], values[:, half:]], axis=0)
+
+
+def unfold(values):
+    half = values.shape[0] // 2
+    return jnp.concatenate([values[:half], values[half:]], axis=1)
+
+
+def split_high_low(values):
+    high = values.astype(jnp.bfloat16).astype(jnp.float32)
+    return high, values - high
+
+
+def mix_kernel(
+    z_count, channels,
+    tokens, gain, conv_base, taps, logit, mats_decay, mats_input, rec_gain, second_gain,
+    rec_state, w_in, w_gate, w_out,
+    residual_out, second_out, state_out, branch_out,
+    xs, v_in, v_gate, v_out, part, from_partner, zsum, from_z,
+    w_sem, gz_send, gp_send, g_recv, p_send, p_recv, rz_send, rz_recv,
+):
+    ep, z, core = places(z_count)
+    other = 1 - core
+    loads = [
+        pltpu.make_async_copy(src, dst, w_sem.at[i])
+        for i, (src, dst) in enumerate(((w_in, v_in), (w_gate, v_gate), (w_out, v_out)))
+    ]
+    for load in loads:
+        load.start()
+    barrier = pltpu.get_barrier_semaphore()
+    pl.semaphore_signal(barrier, inc=1, device_id=(ep, z * 2 + other), device_id_type=MESH)
+    for d in range(1, z_count):
+        pl.semaphore_signal(
+            barrier, inc=1, device_id=(ep, (z + d) % z_count * 2 + core), device_id_type=MESH
+        )
+    width = tokens.shape[1]
+    half = width // 2
+    own = tokens[...].astype(jnp.float32)
+    me = z * 2 + core
+    xs[rows16(me), :] = fold(norm_rows(own, gain[...])).astype(jnp.bfloat16)
+    pl.semaphore_wait(barrier, z_count)
+
+    def to_partner(zz):
+        block = xs.at[rows16(zz * 2 + core), :]
+        return remote(block, block, gp_send.at[zz], g_recv.at[zz * 2 + core], ep, z, other)
+
+    mine = xs.at[rows16(me), :]
+    sent = []
+    for d in range(1, z_count):
+        copy = remote(mine, mine, gz_send.at[d], g_recv.at[me], ep, (z + d) % z_count, core)
+        copy.start()
+        sent.append(copy)
+    copy = to_partner(z)
+    copy.start()
+    sent.append(copy)
+    for d in (1, z_count - 1) + tuple(range(2, z_count - 1)):
+        zz = (z + d) % z_count
+        block = xs.at[rows16(zz * 2 + core), :]
+        remote(block, block, gz_send.at[0], g_recv.at[zz * 2 + core], ep, zz, core).wait_recv()
+        copy = to_partner(zz)
+        copy.start()
+        sent.append(copy)
+    for zz in range(z_count):
+        block = xs.at[rows16(zz * 2 + other), :]
+        remote(block, block, gz_send.at[0], g_recv.at[zz * 2 + other], ep, z, other).wait_recv()
+    for copy in sent:
+        copy.wait_send()
+
+    blocks = 2 * z_count
+    local = w_in.shape[1]
+    rows = blocks * 8
+
+    def project(weights):
+        top = jnp.dot(xs[...], weights[:half], preferred_element_type=jnp.float32)
+        low = jnp.dot(xs[...], weights[half:], preferred_element_type=jnp.float32)
+        top = top.reshape(blocks, 16, local)[:, :8]
+        low = low.reshape(blocks, 16, local)[:, 8:]
+        return (top + low).reshape(rows, local).astype(jnp.bfloat16)
+
+    loads[0].wait()
+    branch_in = project(v_in)
+    loads[1].wait()
+    branch_gate = project(v_gate).astype(jnp.float32)
+    branch_out[...] = branch_in
+    place = pl.ds(pl.multiple_of(me * local, LANES), local)
+    tap = taps[:, place].astype(jnp.float32)
+    conv = conv_base[...] + tap[-1:] * branch_in.astype(jnp.float32)
+    conv_low = conv.astype(jnp.bfloat16)
+    count = local // LANES
+
+    def gates(mats):
+        return jax.nn.sigmoid(
+            jnp.concatenate(
+                [
+                    jnp.dot(
+                        conv_low[:, i * LANES : (i + 1) * LANES],
+                        mats[me * count + i],
+                        preferred_element_type=jnp.float32,
+                    )
+                    for i in range(count)
+                ],
+                axis=1,
+            )
+        )
+
+    lam = logit[:, place]
+    soft = jnp.log(1.0 + jnp.exp(-jnp.abs(lam))) + jnp.maximum(-lam, 0.0)
+    log_keep = -RATE * gates(mats_decay) * soft
+    twice = 2.0 * log_keep
+    near = -twice * (1.0 + twice * (0.5 + twice * (1.0 / 6.0 + twice * (1.0 / 24.0))))
+    rest = jnp.where(twice > -0.03, near, 1.0 - jnp.exp(twice))
+    state = jnp.exp(log_keep) * rec_state[...] + jnp.sqrt(rest) * gates(mats_input) * conv
+    state_out[...] = state
+    hidden = state * jax.nn.gelu(branch_gate)
+    squares = jnp.sum(hidden * hidden, axis=1, keepdims=True)
+    gained = (hidden * rec_gain[:, place].astype(jnp.float32)).astype(jnp.bfloat16)
+    loads[2].wait()
+
+    def store_blocks(columns, top, low):
+        for c in range(2):
+            for zz in range(z_count):
+                b = zz * 2 + c
+                piece = jnp.concatenate([top[b * 8 : b * 8 + 8], low[b * 8 : b * 8 + 8]], axis=0)
+                first = (c * z_count + zz) * 16
+                part[first : first + 16, columns] = piece.astype(jnp.bfloat16)
+
+    step = half // CHUNKS
+    for k in range(CHUNKS):
+        top = jnp.dot(
+            gained, v_out[:, k * step : (k + 1) * step], preferred_element_type=jnp.float32
+        )
+        low = jnp.dot(
+            gained, v_out[:, half + k * step : half + (k + 1) * step],
+            preferred_element_type=jnp.float32,
+        )
+        store_blocks(slice(k * step, (k + 1) * step), top, low)
+    high_sq, low_sq = split_high_low(jnp.broadcast_to(squares, (rows, LANES)))
+    store_blocks(slice(half, half + LANES), high_sq, low_sq)
+
+    copy = remote(
+        part.at[rows16(other * z_count, z_count), :], from_partner, p_send, p_recv, ep, z, other
+    )
+    copy.start()
+    copy.wait()
+    zsum[...] = (
+        part[rows16(core * z_count, z_count), :].astype(jnp.float32)
+        + from_partner[...].astype(jnp.float32)
+    ).astype(jnp.bfloat16)
+    sent = []
+    for d in range(1, z_count):
+        zz = (z + d) % z_count
+        copy = remote(
+            zsum.at[rows16(zz), :], from_z.at[z], rz_send.at[d], rz_recv.at[z], ep, zz, core
+        )
+        copy.start()
+        sent.append(copy)
+    total = zsum[rows16(z), :].astype(jnp.float32)
+    for d in range(1, z_count):
+        zz = (z + d) % z_count
+        remote(
+            zsum.at[rows16(zz), :], from_z.at[zz], rz_send.at[0], rz_recv.at[zz], ep, zz, core
+        ).wait_recv()
+        total = total + from_z[zz].astype(jnp.float32)
+    for copy in sent:
+        copy.wait_send()
+    mix = unfold(total[:, :half])
+    extra = total[:, half:]
+    own_squares = (extra[:8] + extra[8:])[:, :1]
+    residual = own + mix * lax.rsqrt(own_squares / channels + EPS)
+    residual_out[...] = residual
+    second_out[...] = fold(norm_rows(residual, second_gain[...])).astype(jnp.bfloat16)
+
+
+def expert_kernel(
+    z_count, ep_count,
+    second, weights, residual, g_hbm, u_hbm, d_hbm,
+    result_out,
+    xs, vg, vu, vd, chooser, scatter, sel, act, ys, part, from_partner, csum, from_ep, zsum, from_z,
+    g_sem, u_sem, d_sem, gz_send, ge_send, gp_send, g_recv,
+    p_send, p_recv, re_send, re_recv, rz_send, rz_recv,
+):
+    ep, z, core = places(z_count)
+    other = 1 - core
+    experts = g_hbm.shape[0]
+    half = second.shape[1]
+    shards = 2 * ep_count * z_count
+
+    def load_g(e):
+        return pltpu.make_async_copy(g_hbm.at[e], vg.at[e], g_sem.at[e])
+
+    def load_u(e):
+        return pltpu.make_async_copy(u_hbm.at[e], vu.at[e], u_sem.at[e])
+
+    def load_d(e):
+        return pltpu.make_async_copy(d_hbm.at[e], vd.at[e], d_sem.at[e])
+
+    for e in range(experts):
+        load_g(e).start()
+        load_u(e).start()
+    for e in range(experts):
+        load_d(e).start()
+
+    barrier = pltpu.get_barrier_semaphore()
+    pl.semaphore_signal(barrier, inc=1, device_id=(ep, z * 2 + other), device_id_type=MESH)
+    for d in range(1, z_count):
+        pl.semaphore_signal(
+            barrier, inc=1, device_id=(ep, (z + d) % z_count * 2 + core), device_id_type=MESH
+        )
+    for d in range(1, ep_count):
+        pl.semaphore_signal(
+            barrier, inc=1, device_id=((ep + d) % ep_count, z * 2 + core), device_id_type=MESH
+        )
+
+    def shard_of(c, e, zz):
+        return (c * ep_count + e) * z_count + zz
+
+    def block_of(c, e, zz):
+        return xs.at[rows16(shard_of(c, e, zz)), :]
+
+    me = shard_of(core, ep, z)
+    high, low = split_high_low(weights[...])
+    xs[rows16(me), :half] = second[...]
+    xs[rows16(me), half:] = jnp.concatenate([high, low], axis=0).astype(jnp.bfloat16)
+    pl.semaphore_wait(barrier, z_count + ep_count - 1)
+
+    sent = []
+
+    def send(block, send_sem, number, to_ep, to_z, to_core):
+        copy = remote(block, block, send_sem, g_recv.at[number], to_ep, to_z, to_core)
+        copy.start()
+        sent.append(copy)
+
+    def arrived(c, e, zz):
+        block = block_of(c, e, zz)
+        remote(
+            block, block, gz_send.at[0], g_recv.at[shard_of(c, e, zz)], ep, z, other
+        ).wait_recv()
+
+    mine = block_of(core, ep, z)
+    z_order = (1, z_count - 1) + tuple(range(2, z_count - 1))
+    for d in z_order:
+        send(mine, gz_send.at[d], me, ep, (z + d) % z_count, core)
+    for j in range(1, ep_count):
+        send(mine, ge_send.at[0, j], me, (ep + j) % ep_count, z, core)
+    send(mine, gp_send.at[0, 0], me, ep, z, other)
+    for d in z_order:
+        zz = (z + d) % z_count
+        arrived(core, ep, zz)
+        block, number = block_of(core, ep, zz), shard_of(core, ep, zz)
+        for j in range(1, ep_count):
+            send(block, ge_send.at[d, j], number, (ep + j) % ep_count, z, core)
+        send(block, gp_send.at[d, 0], number, ep, z, other)
+    for d in (0,) + z_order:
+        zz = (z + d) % z_count
+        for j in range(1, ep_count):
+            e = (ep + j) % ep_count
+            arrived(core, e, zz)
+            send(block_of(core, e, zz), gp_send.at[d, j], shard_of(core, e, zz), ep, z, other)
+    for e in range(ep_count):
+        for zz in range(z_count):
+            arrived(other, e, zz)
+    for copy in sent:
+        copy.wait_send()
+
+    cap = 2
+    per_expert = shards * cap
+    slots = experts * per_expert
+    rows = shards * 16
+    extra = xs[:, half:].astype(jnp.float32).reshape(shards, 16, LANES)
+    high = jnp.concatenate([extra[:, :8], extra[:, :8]], axis=1).reshape(rows, LANES)
+    low = jnp.concatenate([extra[:, 8:], extra[:, 8:]], axis=1).reshape(rows, LANES)
+    mask = (high > 0.0).astype(jnp.float32)
+    row = lax.broadcasted_iota(jnp.int32, (rows, rows), 0)
+    col = lax.broadcasted_iota(jnp.int32, (rows, rows), 1)
+    earlier = ((row // 8 == col // 8) & (col < row)).astype(jnp.float32).astype(jnp.bfloat16)
+    before = jnp.dot(earlier, mask.astype(jnp.bfloat16), preferred_element_type=jnp.float32)
+    name = lax.broadcasted_iota(jnp.int32, (LANES, slots), 0)
+    lane = lax.broadcasted_iota(jnp.int32, (LANES, slots), 1)
+    spread = (name == ep * experts + lane // per_expert).astype(jnp.float32).astype(jnp.bfloat16)
+
+    def to_slots(values):
+        return jnp.dot(values.astype(jnp.bfloat16), spread, preferred_element_type=jnp.float32)
+
+    row = lax.broadcasted_iota(jnp.int32, (rows, slots), 0)
+    lane = lax.broadcasted_iota(jnp.int32, (rows, slots), 1)
+    wanted = (lane % per_expert - row // 16 * cap).astype(jnp.float32)
+    hit = jnp.where(to_slots(mask) > 0.5, 1.0, 0.0) * jnp.where(to_slots(before) == wanted, 1.0, 0.0)
+    first = (row % 16 < 8).astype(jnp.float32)
+    chooser[0] = (hit * first).T.astype(jnp.bfloat16)
+    chooser[1] = (hit * (1.0 - first)).T.astype(jnp.bfloat16)
+    share = hit * (to_slots(high) + to_slots(low))
+    scatter[...] = (
+        share.reshape(shards, 16, slots)[:, :8].reshape(shards * 8, slots).astype(jnp.bfloat16)
+    )
+
+    tile = 512
+
+    def choose(i, _):
+        at = pl.multiple_of(i * tile, tile)
+        values = xs[:, pl.ds(at, tile)]
+        for h in range(2):
+            sel[:, pl.ds(h * half + at, tile)] = jnp.dot(
+                chooser[h], values, preferred_element_type=jnp.float32
+            ).astype(jnp.bfloat16)
+        return 0
+
+    lax.fori_loop(0, half // tile, choose, 0)
+
+    units = g_hbm.shape[2]
+    piece = min(256, units)
+
+    def run(e, _):
+        load_g(e).wait()
+        load_u(e).wait()
+        at = pl.ds(pl.multiple_of(e * per_expert, per_expert), per_expert)
+        for n in range(units // piece):
+            columns = slice(n * piece, (n + 1) * piece)
+            gate = jnp.dot(sel[at, :], vg[e, :, columns], preferred_element_type=jnp.float32)
+            upper = jnp.dot(sel[at, :], vu[e, :, columns], preferred_element_type=jnp.float32)
+            gate = jnp.minimum(gate, CLAMP)
+            act[at, columns] = (
+                (jnp.clip(upper, -CLAMP, CLAMP) + 1.0) * (gate * jax.nn.sigmoid(ALPHA * gate))
+            ).astype(jnp.bfloat16)
+        return 0
+
+    lax.fori_loop(0, experts, run, 0)
+
+    wide = 2 * half // CHUNKS
+    narrow = wide // 2
+    side = ep_count * z_count
+    held = {}
+
+    def produce(k):
+        def down(e, _):
+            at = pl.ds(pl.multiple_of(e * per_expert, per_expert), per_expert)
+            ys[at, :] = jnp.dot(
+                act[at, :], vd[e, :, k * wide : (k + 1) * wide],
+                preferred_element_type=jnp.float32,
+            ).astype(jnp.bfloat16)
+            return 0
+
+        if k == 0:
+            for e in range(experts):
+                load_d(e).wait()
+        lax.fori_loop(0, experts, down, 0)
+        out = jnp.dot(scatter[...], ys[...], preferred_element_type=jnp.float32)
+        out = out.reshape(shards, 8, wide)
+        out = jnp.concatenate([out[:, :, :narrow], out[:, :, narrow:]], axis=1)
+        part[k] = out.reshape(rows, narrow).astype(jnp.bfloat16)
+        copy = remote(
+            part.at[k, rows16(other * side, side), :], from_partner.at[k],
+            p_send.at[k], p_recv.at[k], ep, z, other,
+        )
+        copy.start()
+        held["p", k] = copy
+
+    def chip_sum(k):
+        held["p", k].wait()
+        csum[k] = (
+            part[k, rows16(core * side, side), :].astype(jnp.float32)
+            + from_partner[k].astype(jnp.float32)
+        ).astype(jnp.bfloat16)
+        for j in range(1, ep_count):
+            e = (ep + j) % ep_count
+            copy = remote(
+                csum.at[k, rows16(e * z_count, z_count), :], from_ep.at[k, ep],
+                re_send.at[k, j], re_recv.at[k, ep], e, z, core,
+            )
+            copy.start()
+            held["e", k, j] = copy
+
+    def group_sum(k):
+        total = csum[k, rows16(ep * z_count, z_count), :].astype(jnp.float32)
+        for j in range(1, ep_count):
+            e = (ep + j) % ep_count
+            remote(
+                csum.at[k, rows16(e * z_count, z_count), :], from_ep.at[k, e],
+                re_send.at[k, 0], re_recv.at[k, e], e, z, core,
+            ).wait_recv()
+            total = total + from_ep[k, e].astype(jnp.float32)
+        zsum[k] = total.astype(jnp.bfloat16)
+        for d in range(1, z_count):
+            zz = (z + d) % z_count
+            copy = remote(
+                zsum.at[k, rows16(zz), :], from_z.at[k, z],
+                rz_send.at[k, d], rz_recv.at[k, z], ep, zz, core,
+            )
+            copy.start()
+            held["z", k, d] = copy
+
+    def finish(k):
+        total = zsum[k, rows16(z), :].astype(jnp.float32)
+        for d in range(1, z_count):
+            zz = (z + d) % z_count
+            remote(
+                zsum.at[k, rows16(zz), :], from_z.at[k, zz],
+                rz_send.at[k, 0], rz_recv.at[k, zz], ep, zz, core,
+            ).wait_recv()
+            total = total + from_z[k, zz].astype(jnp.float32)
+        columns = slice(k * wide, (k + 1) * wide)
+        result_out[:, columns] = (residual[:, columns] + unfold(total)).astype(jnp.bfloat16)
+
+    stages = (produce, chip_sum, group_sum, finish)
+    for step in range(CHUNKS + len(stages) - 1):
+        for lag, stage in enumerate(stages):
+            if 0 <= step - lag < CHUNKS:
+                stage(step - lag)
+    for key, copy in held.items():
+        if key[0] != "p":
+            copy.wait_send()
+
+
+def kernel_plan(
+    tokens, rec_state, conv_state, route_ids, route_weights, first_gain, proj_input, proj_gate,
+    conv_taps, decay_logit, block_decay, block_input, rec_gain, proj_out, second_gain,
+    expert_gate, expert_up, expert_down,
+):
+    tp_count, ep_count = lax.axis_size("tp"), lax.axis_size("ep")
+    tp_place = lax.axis_index("tp")
+    z_count = tp_count // 2
+    own_count, width = tokens.shape
+    half = width // 2
+    seqs, local = rec_state.shape
+    local_experts, _, units = expert_gate.shape
+    bf16, f32 = jnp.bfloat16, jnp.float32
+    taps = lax.dynamic_slice_in_dim(conv_taps, tp_place * local, local, 1).astype(f32)
+    conv_base = jnp.zeros((seqs, local), f32)
+    for tap in range(conv_state.shape[1]):
+        conv_base = conv_base + taps[tap] * conv_state[:, tap].astype(f32)
+    own_ids = lax.dynamic_slice_in_dim(route_ids, tp_place * own_count, own_count, 0)
+    named = own_ids[:, :, None] == jnp.arange(LANES, dtype=jnp.int32)
+    spread_weights = jnp.sum(jnp.where(named, route_weights[:, :, None], 0.0), axis=1)
+
+    vmem = pl.BlockSpec(memory_space=pltpu.VMEM)
+    hbm = pl.BlockSpec(memory_space=pl.ANY)
+    dma = pltpu.SemaphoreType.DMA
+    group = 16 * tp_count
+    residual, second, new_state, branch_in = pl.pallas_call(
+        functools.partial(mix_kernel, z_count, local * tp_count),
+        out_shape=(
+            jax.ShapeDtypeStruct((own_count, width), f32),
+            jax.ShapeDtypeStruct((2 * own_count, half), bf16),
+            jax.ShapeDtypeStruct((seqs, local), f32),
+            jax.ShapeDtypeStruct((seqs, local), bf16),
+        ),
+        in_specs=[vmem] * 10 + [hbm] * 3,
+        out_specs=(vmem,) * 4,
+        scratch_shapes=[
+            pltpu.VMEM((group, half), bf16),
+            pltpu.VMEM((width, local), bf16),
+            pltpu.VMEM((width, local), bf16),
+            pltpu.VMEM((local, width), bf16),
+            pltpu.VMEM((group, half + LANES), bf16),
+            pltpu.VMEM((group // 2, half + LANES), bf16),
+            pltpu.VMEM((group // 2, half + LANES), bf16),
+            pltpu.VMEM((z_count, 16, half + LANES), bf16),
+            dma((3,)), dma((z_count,)), dma((z_count,)), dma((tp_count,)),
+            dma, dma, dma((z_count,)), dma((z_count,)),
+        ],
+        compiler_params=pltpu.CompilerParams(
+            collective_id=0, has_side_effects=True, vmem_limit_bytes=40_000_000
+        ),
+        name="mix",
+    )(
+        tokens, first_gain[None], conv_base, conv_taps, decay_logit[None], block_decay,
+        block_input, rec_gain[None], second_gain[None], rec_state, proj_input, proj_gate, proj_out,
+    )
+    new_conv = jnp.concatenate([conv_state[:, 1:], branch_in[:, None, :]], axis=1)
+
+    shards = tp_count * ep_count
+    rows = shards * 16
+    side = rows // 2
+    slots = local_experts * shards * 2
+    wide = width // CHUNKS
+    narrow = wide // 2
+    result = pl.pallas_call(
+        functools.partial(expert_kernel, z_count, ep_count),
+        out_shape=jax.ShapeDtypeStruct((own_count, width), bf16),
+        in_specs=[vmem] * 3 + [hbm] * 3,
+        out_specs=vmem,
+        scratch_shapes=[
+            pltpu.VMEM((rows, half + LANES), bf16),
+            pltpu.VMEM((local_experts, width, units), bf16),
+            pltpu.VMEM((local_experts, width, units), bf16),
+            pltpu.VMEM((local_experts, units, width), bf16),
+            pltpu.VMEM((2, slots, rows), bf16),
+            pltpu.VMEM((shards * 8, slots), bf16),
+            pltpu.VMEM((slots, width), bf16),
+            pltpu.VMEM((slots, units), bf16),
+            pltpu.VMEM((slots, wide), bf16),
+            pltpu.VMEM((CHUNKS, rows, narrow), bf16),
+            pltpu.VMEM((CHUNKS, side, narrow), bf16),
+            pltpu.VMEM((CHUNKS, side, narrow), bf16),
+            pltpu.VMEM((CHUNKS, ep_count, 16 * z_count, narrow), bf16),
+            pltpu.VMEM((CHUNKS, 16 * z_count, narrow), bf16),
+            pltpu.VMEM((CHUNKS, z_count, 16, narrow), bf16),
+            dma((local_experts,)), dma((local_experts,)), dma((local_experts,)),
+            dma((z_count,)), dma((z_count, ep_count)), dma((z_count, ep_count)), dma((shards,)),
+            dma((CHUNKS,)), dma((CHUNKS,)),
+            dma((CHUNKS, ep_count)), dma((CHUNKS, ep_count)),
+            dma((CHUNKS, z_count)), dma((CHUNKS, z_count)),
+        ],
+        compiler_params=pltpu.CompilerParams(
+            collective_id=1, has_side_effects=True, vmem_limit_bytes=VMEM_LIMIT
+        ),
+        name="experts",
+    )(second, spread_weights, residual, expert_gate, expert_up, expert_down)
+    return (result, new_state, new_conv)
+
+
+def per_device(*args):
+    tokens, rec_state, ids, block = args[0], args[1], args[3], args[10]
+    tp_count, ep_count = lax.axis_size("tp"), lax.axis_size("ep")
+    shards = tp_count * ep_count
+    expert_rows = args[15].shape[0] * shards * 2
+    fits = (
+        tokens.shape[0] == 8
+        and tp_count % 2 == 0
+        and tp_count >= 8
+        and max(2, tokens.shape[0] * ids.shape[1] // EXPERTS) == 2
+        and expert_rows <= 256
+        and block.shape[1] == LANES
+        and rec_state.shape[1] % LANES == 0
+    )
+    return kernel_plan(*args) if fits else collective_plan(*args)
+
+
 def solution(mesh):
     in_specs = (
         P(("ep", "tp"), None),

time: 197 us -> 97.5 us (0.49)
  waiting for transfers between devices: 79.8 us -> 0 us
  Pallas kernels: 0 us -> 76.2 us
  blocking collectives: 42.7 us -> 0 us
  matrix products: 36.8 us -> 0 us
  between operations: 14.6 us -> 0.69 us
  local copies, waits for them, and re-layouts: 10.3 us -> 16.4 us
  other arithmetic: 8.29 us -> 3.5 us
  starting transfers between devices: 3.84 us -> 0 us
    pallas_call x0 -> x2, Pallas kernels: none -> 76.2 us  [the longest x1 53.9 us: kernel_plan(): pl.pallas_call(functools.partial(expert_kernel, z_count, ep_count), out_s...]
    dot_general x9 -> x0, matrix products: 36.8 us -> none  [the longest x1 17.8 us: run_experts(): jnp.einsum('erf,efd->erd', act, expert_down, preferred_element_type=jnp.f...]
    unnamed x4 -> x0, waiting for transfers between devices: 35.6 us -> none
    all_gather x1 -> x0, waiting for transfers between devices: 26.3 us -> none  [per_device(): lax.all_gather(arrived, 'tp', axis=1, tiled=True)]
    unnamed x1 -> x0, blocking collectives: 17 us -> none
    all_gather x1 -> x0, blocking collectives: 16.5 us -> none  [per_device(): piece = lax.all_gather(normed, 'tp', axis=0, tiled=True)]
    reduce_scatter x1 -> x0, waiting for transfers between devices: 13.2 us -> none  [per_device(): lax.psum_scatter(partial_value.astype(jnp.bfloat16), 'tp', scatter_dimens...]
    all_to_all x1 -> x0, blocking collectives: 9.19 us -> none  [per_device(): lax.all_to_all(outgoing, 'ep', split_axis=0, concat_axis=1, tiled=True)]
  transfers between devices with their start and end apart: 4 -> 0, of which waited for: 4 -> 0; matrix products, arithmetic and copies ran while one was open for 1% -> 0% of each run, Pallas kernels for 0% -> 0%
where the time goes in v1:
time: 97.5 us; the launch traced here: 96.7 us
  Pallas kernels  76.2 us (78%)
  local copies, waits for them, and re-layouts  16.4 us (17%)
  other arithmetic  3.5 us (4%)
    pallas_call x1, Pallas kernels, kernel_plan(): pl.pallas_call(functools.partial(expert_kernel, z_count, ep_count), out_s...  53.9 us
    pallas_call x1, Pallas kernels, kernel_plan(): pl.pallas_call(functools.partial(mix_kernel, z_count, local * tp_count),...  22.3 us
    unnamed x26, local copies, waits for them, and re-layouts  13.3 us

profile of v1, /device:TPU:0, one launch (start us, length us, event | category | flops | bytes accessed | tf_op | source)
XLA Modules:
  0.0 96.7 jit_solution(4661857830250144806)
XLA Ops:
  0.6 0.0 copy-start
  0.6 0.7 dynamic-slice_convert_fusion
  1.3 0.8 fusion.conv_base
  2.2 0.7 broadcast_in_dim.30.gain
  2.9 0.7 broadcast_in_dim.33.second_gain
  3.6 0.7 broadcast_in_dim.32.rec_gain
  4.3 0.0 copy-start.1
  4.3 1.6 %copy-done.1 = bf16[4096,256]{1,0:T(8,128)(2,1)S(1)} copy-done((bf16[4096,256]{1,0:T(8,128)(2,1)S(1)}, bf16[4096,256]{1,0:T(8,128)(2,1)}, u32[]{:S(2)}) %copy-start.1) | copy-done | bytes 2097176
  5.9 0.0 copy-start.2
  5.9 1.6 %copy-done.2 = bf16[4096,256]{1,0:T(8,128)(2,1)S(1)} copy-done((bf16[4096,256]{1,0:T(8,128)(2,1)S(1)}, bf16[4096,256]{1,0:T(8,128)(2,1)}, u32[]{:S(2)}) %copy-start.2) | copy-done | bytes 2097176
  7.5 0.0 copy-start.3
  7.5 1.6 %copy-done.3 = bf16[256,4096]{1,0:T(8,128)(2,1)S(1)} copy-done((bf16[256,4096]{1,0:T(8,128)(2,1)S(1)}, bf16[256,4096]{1,0:T(8,128)(2,1)}, u32[]{:S(2)}) %copy-start.3) | copy-done | bytes 2097176
  9.1 0.0 copy-start.4
  9.1 1.0 %copy-done.4 = bf16[16,128,128]{2,1,0:T(8,128)(2,1)S(1)} copy-done((bf16[16,128,128]{2,1,0:T(8,128)(2,1)S(1)}, bf16[16,128,128]{2,1,0:T(8,128)(2,1)}, u32[]{:S(2)}) %copy-start.4) | copy-done | bytes 524312
  10.1 0.0 copy-start.5
  10.1 1.0 %copy-done.5 = bf16[16,128,128]{2,1,0:T(8,128)(2,1)S(1)} copy-done((bf16[16,128,128]{2,1,0:T(8,128)(2,1)S(1)}, bf16[16,128,128]{2,1,0:T(8,128)(2,1)}, u32[]{:S(2)}) %copy-start.5) | copy-done | bytes 524312
  11.1 0.0 copy-start.8
  11.1 0.8 copy-done.8
  12.0 0.0 copy-start.9
  12.0 0.8 copy-done.9
  12.8 0.0 copy-start.10
  12.8 0.7 copy-done.10
  13.5 0.0 copy-start.11
  13.5 0.7 copy-done.11
  14.2 22.3 %mix.1 = (f32[8,4096]{1,0:T(8,128)S(1)}, bf16[16,2048]{1,0:T(8,128)(2,1)S(1)}, f32[64,256]{1,0:T(8,128)S(1)}, bf16[64,256]{1,0:T(8,128)(2,1)S(1)}) custom-call(bf16[8,4096]{1,0:T(8,128)(2,1)S(1)} %copy-done.8, bf16[1,4096]{1,0:T(2,128)(2,1)S(1)} %broadcast_in_dim.30.gain, f32[64,256]{1,0:T(8,128)S(1)} %fusion.conv_base, bf16[4,2048]{1,0:T(4,128)(2,1)S(1)} %copy-done.10, ...), custom_call_target="tpu_custom_call" | custom-call | tf_op jit(solution)/shard_map/mix/pallas_call | solution.py:623
  36.5 0.0 copy-start.6
  36.6 0.6 copy-done.6
  37.2 0.0 copy-start.7
  37.2 0.6 copy-done.7
  37.8 0.0 copy-done
  37.8 0.1 constant_dynamic-slice_fusion
  37.9 1.4 %select_reduce_fusion.weights = f32[8,128]{1,0:T(8,128)} fusion(f32[8,4]{0,1:T(4,128)} %param.22, s32[8,4]{0,1:T(4,128)S(1)} %constant_dynamic-slice_fusion), kind=kLoop, calls=%fused_computation.6 | loop fusion | flops 11264 | bytes 4352 | tf_op jit(solution)/shard_map/reduce_sum | solution.py:617
  39.2 53.9 %experts.1 = bf16[8,4096]{1,0:T(8,128)(2,1)} custom-call(bf16[16,2048]{1,0:T(8,128)(2,1)} %copy-done.7, f32[8,128]{1,0:T(8,128)} %select_reduce_fusion.weights, f32[8,4096]{1,0:T(8,128)} %copy-done.6, bf16[4,4096,512]{2,1,0:T(8,128)(2,1)} %g_hbm.1, bf16[4,4096,512]{2,1,0:T(8,128)(2,1)} %u_hbm.1, bf16[4,512,4096]{2,1,0:T(8,128)(2,1)} %d_hbm.1), custom_call_target="tpu_custom_call" | custom-call | tf_op jit(solution)/shard_map/experts/pallas_call | solution.py:661
  93.1 0.8 slice.27
  94.0 0.7 pad_maximum_fusion
  94.6 1.5 %copy.25 = bf16[8,4096]{1,0:T(8,128)(2,1)} copy(bf16[8,4096]{1,0:T(8,128)(2,1)} %experts.1) | data formatting | bytes 131072
  96.1 0.6 copy.26
  (1 shorter events, 0.0 us)
Async XLA Ops:
  0.6 37.2 %copy-start = (s32[64,4]{0,1:T(4,128)S(1)}, s32[64,4]{0,1:T(4,128)}, u32[]{:S(2)}) copy-start(s32[64,4]{0,1:T(4,128)} %param.21) | copy-start | bytes 3076
  4.3 1.6 %copy-start.1 = (bf16[4096,256]{1,0:T(8,128)(2,1)S(1)}, bf16[4096,256]{1,0:T(8,128)(2,1)}, u32[]{:S(2)}) copy-start(bf16[4096,256]{1,0:T(8,128)(2,1)} %w_in.1) | copy-start | bytes 6291460
  5.9 1.6 %copy-start.2 = (bf16[4096,256]{1,0:T(8,128)(2,1)S(1)}, bf16[4096,256]{1,0:T(8,128)(2,1)}, u32[]{:S(2)}) copy-start(bf16[4096,256]{1,0:T(8,128)(2,1)} %w_gate.1) | copy-start | bytes 6291460
  7.5 1.6 %copy-start.3 = (bf16[256,4096]{1,0:T(8,128)(2,1)S(1)}, bf16[256,4096]{1,0:T(8,128)(2,1)}, u32[]{:S(2)}) copy-start(bf16[256,4096]{1,0:T(8,128)(2,1)} %w_out.1) | copy-start | bytes 6291460
  9.1 1.0 %copy-start.4 = (bf16[16,128,128]{2,1,0:T(8,128)(2,1)S(1)}, bf16[16,128,128]{2,1,0:T(8,128)(2,1)}, u32[]{:S(2)}) copy-start(bf16[16,128,128]{2,1,0:T(8,128)(2,1)} %mats_decay.1) | copy-start | bytes 1572868
  10.1 1.0 %copy-start.5 = (bf16[16,128,128]{2,1,0:T(8,128)(2,1)S(1)}, bf16[16,128,128]{2,1,0:T(8,128)(2,1)}, u32[]{:S(2)}) copy-start(bf16[16,128,128]{2,1,0:T(8,128)(2,1)} %mats_input.1) | copy-start | bytes 1572868
  11.1 0.8 copy-start.8
  12.0 0.8 copy-start.9
  12.8 0.7 copy-start.10
  13.5 0.7 copy-start.11
  36.5 0.6 copy-start.6
  37.2 0.6 copy-start.7

commit v2 on v1

--- a/solution.py
+++ b/solution.py
@@ -198,14 +198,29 @@
 
 def mix_kernel(
     z_count, channels,
-    tokens, gain, conv_base, taps, logit, mats_decay, mats_input, rec_gain, second_gain,
-    rec_state, w_in, w_gate, w_out,
-    residual_out, second_out, state_out, branch_out,
-    xs, v_in, v_gate, v_out, part, from_partner, zsum, from_z,
+    gain, logit, rec_gain, second_gain,
+    tokens_hbm, conv_hbm, taps_hbm, decay_hbm, input_hbm, state_hbm, w_in, w_gate, w_out,
+    residual_out, second_out, state_out, conv_out,
+    tokens, old_conv, taps, mats_decay, mats_input, rec_state, small_sem, xs, v_in, v_gate, v_out, part, from_partner, zsum, from_z,
     w_sem, gz_send, gp_send, g_recv, p_send, p_recv, rz_send, rz_recv,
 ):
     ep, z, core = places(z_count)
     other = 1 - core
+    me = z * 2 + core
+    count = mats_decay.shape[0]
+    at_blocks = pl.ds(me * count, count)
+    small = [
+        pltpu.make_async_copy(src, dst, small_sem.at[i])
+        for i, (src, dst) in enumerate(
+            (
+                (tokens_hbm, tokens), (conv_hbm, old_conv), (taps_hbm, taps),
+                (decay_hbm.at[at_blocks], mats_decay), (input_hbm.at[at_blocks], mats_input),
+                (state_hbm, rec_state),
+            )
+        )
+    ]
+    for load in small:
+        load.start()
     loads = [
         pltpu.make_async_copy(src, dst, w_sem.at[i])
         for i, (src, dst) in enumerate(((w_in, v_in), (w_gate, v_gate), (w_out, v_out)))
@@ -220,9 +235,9 @@
         )
     width = tokens.shape[1]
     half = width // 2
+    small[0].wait()
     own = tokens[...].astype(jnp.float32)
-    me = z * 2 + core
-    xs[rows16(me), :] = fold(norm_rows(own, gain[...])).astype(jnp.bfloat16)
+    xs[rows16(me), :] = fold(norm_rows(own, gain[...].astype(jnp.float32).reshape(1, width))).astype(jnp.bfloat16)
     pl.semaphore_wait(barrier, z_count)
 
     def to_partner(zz):
@@ -266,12 +281,18 @@
     branch_in = project(v_in)
     loads[1].wait()
     branch_gate = project(v_gate).astype(jnp.float32)
-    branch_out[...] = branch_in
+    for load in small[1:]:
+        load.wait()
+    kept = old_conv.shape[0]
+    for i in range(kept - 1):
+        conv_out[i] = old_conv[i + 1]
+    conv_out[kept - 1] = branch_in
     place = pl.ds(pl.multiple_of(me * local, LANES), local)
     tap = taps[:, place].astype(jnp.float32)
-    conv = conv_base[...] + tap[-1:] * branch_in.astype(jnp.float32)
+    conv = tap[-1:] * branch_in.astype(jnp.float32)
+    for i in range(kept):
+        conv = conv + tap[i : i + 1] * old_conv[i].astype(jnp.float32)
     conv_low = conv.astype(jnp.bfloat16)
-    count = local // LANES
 
     def gates(mats):
         return jax.nn.sigmoid(
@@ -279,7 +300,7 @@
                 [
                     jnp.dot(
                         conv_low[:, i * LANES : (i + 1) * LANES],
-                        mats[me * count + i],
+                        mats[i],
                         preferred_element_type=jnp.float32,
                     )
                     for i in range(count)
@@ -353,14 +374,14 @@
     own_squares = (extra[:8] + extra[8:])[:, :1]
     residual = own + mix * lax.rsqrt(own_squares / channels + EPS)
     residual_out[...] = residual
-    second_out[...] = fold(norm_rows(residual, second_gain[...])).astype(jnp.bfloat16)
+    second_out[...] = fold(norm_rows(residual, second_gain[...].astype(jnp.float32).reshape(1, width))).astype(jnp.bfloat16)
 
 
 def expert_kernel(
     z_count, ep_count,
-    second, weights, residual, g_hbm, u_hbm, d_hbm,
+    weights, second, residual_hbm, g_hbm, u_hbm, d_hbm,
     result_out,
-    xs, vg, vu, vd, chooser, scatter, sel, act, ys, part, from_partner, csum, from_ep, zsum, from_z,
+    residual, small_sem, xs, vg, vu, vd, chooser, scatter, sel, act, ys, part, from_partner, csum, from_ep, zsum, from_z,
     g_sem, u_sem, d_sem, gz_send, ge_send, gp_send, g_recv,
     p_send, p_recv, re_send, re_recv, rz_send, rz_recv,
 ):
@@ -370,6 +391,13 @@
     half = second.shape[1]
     shards = 2 * ep_count * z_count
 
+    own_place = (core * ep_count + ep) * z_count + z
+    own_rows = pltpu.make_async_copy(
+        second, xs.at[rows16(own_place), pl.ds(0, half)], small_sem.at[0]
+    )
+    own_rows.start()
+    own_residual = pltpu.make_async_copy(residual_hbm, residual, small_sem.at[1])
+
     def load_g(e):
         return pltpu.make_async_copy(g_hbm.at[e], vg.at[e], g_sem.at[e])
 
@@ -404,8 +432,9 @@
 
     me = shard_of(core, ep, z)
     high, low = split_high_low(weights[...])
-    xs[rows16(me), :half] = second[...]
     xs[rows16(me), half:] = jnp.concatenate([high, low], axis=0).astype(jnp.bfloat16)
+    own_rows.wait()
+    own_residual.start()
     pl.semaphore_wait(barrier, z_count + ep_count - 1)
 
     sent = []
@@ -574,6 +603,8 @@
             held["z", k, d] = copy
 
     def finish(k):
+        if k == 0:
+            own_residual.wait()
         total = zsum[k, rows16(z), :].astype(jnp.float32)
         for d in range(1, z_count):
             zz = (z + d) % z_count
@@ -608,10 +639,7 @@
     seqs, local = rec_state.shape
     local_experts, _, units = expert_gate.shape
     bf16, f32 = jnp.bfloat16, jnp.float32
-    taps = lax.dynamic_slice_in_dim(conv_taps, tp_place * local, local, 1).astype(f32)
-    conv_base = jnp.zeros((seqs, local), f32)
-    for tap in range(conv_state.shape[1]):
-        conv_base = conv_base + taps[tap] * conv_state[:, tap].astype(f32)
+    kept = conv_state.shape[1]
     own_ids = lax.dynamic_slice_in_dim(route_ids, tp_place * own_count, own_count, 0)
     named = own_ids[:, :, None] == jnp.arange(LANES, dtype=jnp.int32)
     spread_weights = jnp.sum(jnp.where(named, route_weights[:, :, None], 0.0), axis=1)
@@ -620,17 +648,24 @@
     hbm = pl.BlockSpec(memory_space=pl.ANY)
     dma = pltpu.SemaphoreType.DMA
     group = 16 * tp_count
-    residual, second, new_state, branch_in = pl.pallas_call(
+    residual, second, new_state, conv_major = pl.pallas_call(
         functools.partial(mix_kernel, z_count, local * tp_count),
         out_shape=(
             jax.ShapeDtypeStruct((own_count, width), f32),
             jax.ShapeDtypeStruct((2 * own_count, half), bf16),
             jax.ShapeDtypeStruct((seqs, local), f32),
-            jax.ShapeDtypeStruct((seqs, local), bf16),
+            jax.ShapeDtypeStruct((kept, seqs, local), bf16),
         ),
-        in_specs=[vmem] * 10 + [hbm] * 3,
+        in_specs=[vmem] * 4 + [hbm] * 9,
         out_specs=(vmem,) * 4,
         scratch_shapes=[
+            pltpu.VMEM((own_count, width), bf16),
+            pltpu.VMEM((kept, seqs, local), bf16),
+            pltpu.VMEM(conv_taps.shape, bf16),
+            pltpu.VMEM((local // LANES, LANES, LANES), bf16),
+            pltpu.VMEM((local // LANES, LANES, LANES), bf16),
+            pltpu.VMEM((seqs, local), f32),
+            dma((6,)),
             pltpu.VMEM((group, half), bf16),
             pltpu.VMEM((width, local), bf16),
             pltpu.VMEM((width, local), bf16),
@@ -643,14 +678,15 @@
             dma, dma, dma((z_count,)), dma((z_count,)),
         ],
         compiler_params=pltpu.CompilerParams(
-            collective_id=0, has_side_effects=True, vmem_limit_bytes=40_000_000
+            collective_id=0, has_side_effects=True, vmem_limit_bytes=VMEM_LIMIT
         ),
         name="mix",
     )(
-        tokens, first_gain[None], conv_base, conv_taps, decay_logit[None], block_decay,
-        block_input, rec_gain[None], second_gain[None], rec_state, proj_input, proj_gate, proj_out,
-    )
-    new_conv = jnp.concatenate([conv_state[:, 1:], branch_in[:, None, :]], axis=1)
+        first_gain, decay_logit[None], rec_gain[None], second_gain,
+        tokens, jnp.transpose(conv_state, (1, 0, 2)), conv_taps, block_decay, block_input,
+        rec_state, proj_input, proj_gate, proj_out,
+    )
+    new_conv = jnp.transpose(conv_major, (1, 0, 2))
 
     shards = tp_count * ep_count
     rows = shards * 16
@@ -661,9 +697,11 @@
     result = pl.pallas_call(
         functools.partial(expert_kernel, z_count, ep_count),
         out_shape=jax.ShapeDtypeStruct((own_count, width), bf16),
-        in_specs=[vmem] * 3 + [hbm] * 3,
+        in_specs=[vmem] + [hbm] * 5,
         out_specs=vmem,
         scratch_shapes=[
+            pltpu.VMEM((own_count, width), f32),
+            dma((2,)),
             pltpu.VMEM((rows, half + LANES), bf16),
             pltpu.VMEM((local_experts, width, units), bf16),
             pltpu.VMEM((local_experts, width, units), bf16),
@@ -689,7 +727,7 @@
             collective_id=1, has_side_effects=True, vmem_limit_bytes=VMEM_LIMIT
         ),
         name="experts",
-    )(second, spread_weights, residual, expert_gate, expert_up, expert_down)
+    )(spread_weights, second, residual, expert_gate, expert_up, expert_down)
     return (result, new_state, new_conv)
 
 

time: 97.5 us -> 95.8 us (0.983)
  Pallas kernels: 76.2 us -> 87.8 us
  local copies, waits for them, and re-layouts: 16.4 us -> 5.63 us
  other arithmetic: 3.5 us -> 1.35 us
    pallas_call x1, Pallas kernels: 53.9 us -> 64.4 us  [kernel_plan(): pl.pallas_call(functools.partial(expert_kernel, z_count, ep_count), out_s...]
    unnamed x26 -> x7, local copies, waits for them, and re-layouts: 13.3 us -> 4.27 us
    broadcast_in_dim x2 -> x0, local copies, waits for them, and re-layouts: 1.42 us -> none  [the longest x1 0.71 us: kernel_plan(): first_gain[None]]
    pallas_call x1, Pallas kernels: 22.3 us -> 23.5 us  [kernel_plan(): pl.pallas_call(functools.partial(mix_kernel, z_count, local * tp_count),...]
where the time goes in v2:
time: 95.8 us; the launch traced here: 95.5 us
  Pallas kernels  87.8 us (92%)
  local copies, waits for them, and re-layouts  5.63 us (6%)
  other arithmetic  1.35 us (1%)
    pallas_call x1, Pallas kernels, kernel_plan(): pl.pallas_call(functools.partial(expert_kernel, z_count, ep_count), out_s...  64.4 us
    pallas_call x1, Pallas kernels, kernel_plan(): pl.pallas_call(functools.partial(mix_kernel, z_count, local * tp_count),...  23.5 us
    unnamed x7, local copies, waits for them, and re-layouts  4.27 us

profile of v2, /device:TPU:0, one launch (start us, length us, event | category | flops | bytes accessed | tf_op | source)
XLA Modules:
  0.0 95.5 jit_solution(8933375159201331126)
XLA Ops:
  0.6 0.0 copy-start
  0.6 0.7 copy-done
  1.3 0.1 constant_dynamic-slice_fusion
  1.4 1.4 %select_reduce_fusion.weights = f32[8,128]{1,0:T(8,128)} fusion(f32[8,4]{0,1:T(4,128)} %param.22, s32[8,4]{0,1:T(4,128)S(1)} %constant_dynamic-slice_fusion), kind=kLoop, calls=%fused_computation | loop fusion | flops 11264 | bytes 4352 | tf_op jit(solution)/shard_map/reduce_sum | solution.py:645
  2.7 1.3 %broadcast_in_dim.24.rec_gain = bf16[1,2048]{1,0:T(2,128)(2,1)} reshape(bf16[2048]{0:T(1024)(128)(2,1)} %param.30) | data formatting | bytes 8192 | tf_op jit(solution)/shard_map/broadcast_in_dim | solution.py:685
  4.0 23.5 %mix.1 = (f32[8,4096]{1,0:T(8,128)}, bf16[16,2048]{1,0:T(8,128)(2,1)}, f32[64,256]{1,0:T(8,128)}, bf16[3,64,256]{2,1,0:T(8,128)(2,1)}) custom-call(bf16[4096]{0:T(1024)(128)(2,1)} %gain.1, f32[1,2048]{1,0:T(1,128)} %bitcast.5, bf16[1,2048]{1,0:T(2,128)(2,1)} %broadcast_in_dim.24.rec_gain, bf16[4096]{0:T(1024)(128)(2,1)} %second_gain.1, ...), custom_call_target="tpu_custom_call" | custom-call | tf_op jit(solution)/shard_map/mix/pallas_call | solution.py:651
  27.5 0.0 copy-start.1
  27.5 64.4 %experts.1 = bf16[8,4096]{1,0:T(8,128)(2,1)} custom-call(f32[8,128]{1,0:T(8,128)} %select_reduce_fusion.weights, bf16[16,2048]{1,0:T(8,128)(2,1)} %get-tuple-element.7.second, f32[8,4096]{1,0:T(8,128)} %get-tuple-element.8.residual_hbm, bf16[4,4096,512]{2,1,0:T(8,128)(2,1)} %g_hbm.1, bf16[4,4096,512]{2,1,0:T(8,128)(2,1)} %u_hbm.1, bf16[4,512,4096]{2,1,0:T(8,128)(2,1)} %d_hbm.1), custom_call_target="tpu_custom_call" | custom-call | tf_op jit(solution)/shard_map/experts/pallas_call | solution.py:697
  91.9 1.5 %copy.26 = bf16[8,4096]{1,0:T(8,128)(2,1)} copy(bf16[8,4096]{1,0:T(8,128)(2,1)} %experts.1) | data formatting | bytes 131072
  93.4 1.5 %copy.27 = f32[64,256]{1,0:T(8,128)} copy(f32[64,256]{1,0:T(8,128)} %get-tuple-element.15) | data formatting | bytes 131072
  94.8 0.0 copy-done.1
  94.8 0.6 copy.28
Async XLA Ops:
  0.6 0.7 copy-start
  27.5 67.3 %copy-start.1 = (bf16[3,64,256]{2,1,0:T(8,128)(2,1)S(1)}, bf16[3,64,256]{2,1,0:T(8,128)(2,1)}, u32[]{:S(2)}) copy-start(bf16[3,64,256]{2,1,0:T(8,128)(2,1)} %get-tuple-element.10) | copy-start | bytes 294916
